TPU v7x, 32 devices: a whole 2x2x4 slice. The times are simulated.
32 devices in a mesh: kv: 8 (over z, x), tp: 4 (over y, core).
Axes of the slice: x: 2, y: 2, z: 4, core: 2. Of those that a mesh axis runs over, the one named last changes fastest.
Arguments:
- hidden_in: bfloat16 [16, 4096], P(None, ('kv', 'tp')), may hold values from -5 to 5
- pre_gain: float32 [4096], P('kv'), may hold values from 0.1 to 1.9
- w_query: bfloat16 [4096, 3072], P('kv', 'tp'), may hold values from -0.09375 to 0.09375
- w_key: bfloat16 [4096, 1024], P('kv', 'tp'), may hold values from -0.09375 to 0.09375
- w_value: bfloat16 [4096, 1024], P('kv', 'tp'), may hold values from -0.09375 to 0.09375
- w_forget: bfloat16 [4096, 16], P('kv'), may hold values from -0.09375 to 0.09375
- forget_bias: float32 [16], P('tp'), may hold values from -2 to 1.5
- key_cache: bfloat16 [16, 8192, 1024], P(None, 'kv', 'tp'), may hold values from -1300 to 1300
- value_cache: bfloat16 [16, 8192, 1024], P(None, 'kv', 'tp'), may hold values from -6 to 6
- decay_to_end: float32 [16, 16, 8192], P(None, 'tp', 'kv'), may hold values from -8194 to 0, as said below
- w_output: bfloat16 [3072, 4096], P('tp', 'kv'), may hold values from -0.109375 to 0.109375
- mid_gain: float32 [4096], P('kv'), may hold values from 0.1 to 1.9
- w_gate: bfloat16 [4096, 11264], P('kv', 'tp'), may hold values from -0.09375 to 0.09375
- w_up: bfloat16 [4096, 11264], P('kv', 'tp'), may hold values from -0.09375 to 0.09375
- w_down: bfloat16 [11264, 4096], P('tp', 'kv'), may hold values from -0.0546875 to 0.0546875
Outputs:
- updated: float32 [16, 4096], P(None, ('kv', 'tp'))
Inputs may be any that keep to these rules, and one draw needn't show every extreme that they name: `decay_to_end`: never falls toward later positions and is 0 at the last cached position.
All inputs are finite; a program needn't handle non-finite values.
Results may differ from a plain program's by a relative error of at most 0.028.
Values may be sent and summed in bfloat16 or wider, within the bound.
A program may use at most 128 MiB of HBM per device.

v0:
```python
import jax
import jax.numpy as jnp
from jax import lax
from jax.sharding import PartitionSpec as P

D = 4096
QH = 48
KEY_VALUE_HEADS = 16
HD = 64


norm_eps = 1e-06


def combined_all(part, axis, combine):
    gathered = jax.tree.map(lambda a: lax.all_gather(a, axis), part)

    def take(source):
        return jax.tree.map(lambda a: lax.dynamic_index_in_dim(a, source, 0, False), gathered)

    return lax.fori_loop(
        1, lax.axis_size(axis), lambda source, state: combine(state, take(source)), take(0)
    )


def combine_parts(first, second):
    max_first, sum_first, acc_first = first
    max_second, sum_second, acc_second = second
    larger = jnp.maximum(max_first, max_second)
    scale_first = jnp.exp(max_first - larger)
    scale_second = jnp.exp(max_second - larger)
    return (
        larger,
        sum_first * scale_first + sum_second * scale_second,
        acc_first * scale_first[..., None] + acc_second * scale_second[..., None],
    )


def project_block(scaled, w_query, w_key, w_value, w_forget):
    q_part = jnp.dot(scaled, w_query, preferred_element_type=jnp.float32)
    k_part = jnp.dot(scaled, w_key, preferred_element_type=jnp.float32)
    v_part = jnp.dot(scaled, w_value, preferred_element_type=jnp.float32)
    f_part = jnp.dot(scaled, w_forget, preferred_element_type=jnp.float32)
    return (q_part, k_part, v_part, f_part)


def on_device(
    hidden_in,
    pre_gain,
    w_query,
    w_key,
    w_value,
    w_forget,
    forget_bias,
    key_cache,
    value_cache,
    decay_to_end,
    w_output,
    mid_gain,
    w_gate,
    w_up,
    w_down,
):
    batch_rows = hidden_in.shape[0]
    kv_here = decay_to_end.shape[1]
    positions = decay_to_end.shape[2]
    group_size = QH // KEY_VALUE_HEADS
    tp_pos = lax.axis_index("tp")
    col_block = lax.all_gather(hidden_in, "tp", axis=1, tiled=True).astype(jnp.float32)
    scaled = (col_block * pre_gain).astype(jnp.bfloat16)
    square = jnp.sum(col_block * col_block, axis=1, keepdims=True)
    q_part, k_part, v_part, f_part = project_block(scaled, w_query, w_key, w_value, w_forget)
    q_sum, k_sum, v_sum, f_sum, square_all = lax.psum(
        (q_part, k_part, v_part, f_part, square), "kv"
    )
    inv_rms = lax.rsqrt(square_all / D + norm_eps)
    query = (q_sum * inv_rms).astype(jnp.bfloat16).reshape(batch_rows, kv_here, group_size, HD)
    key_new = (k_sum * inv_rms).astype(jnp.bfloat16).reshape(batch_rows, kv_here, HD)
    value_new = (v_sum * inv_rms).astype(jnp.bfloat16).reshape(batch_rows, kv_here, HD)
    forget_mine = lax.dynamic_slice_in_dim(f_sum * inv_rms, tp_pos * kv_here, kv_here, 1)
    log_new = jax.nn.log_sigmoid(forget_mine + forget_bias)
    score_scale = HD ** (-0.5)
    key_rows = key_cache.reshape(batch_rows, positions, kv_here, HD)
    value_rows = value_cache.reshape(batch_rows, positions, kv_here, HD)
    scores = (
        jnp.einsum("bgqd,bpgd->bgqp", query, key_rows, preferred_element_type=jnp.float32)
        * score_scale
    )
    scores = scores + log_new[:, :, None, None] + decay_to_end[:, :, None, :]
    local_max = jnp.max(scores, axis=3)
    weights = jnp.exp(scores - local_max[..., None])
    local_sum = jnp.sum(weights, axis=3)
    local_acc = jnp.einsum(
        "bgqp,bpgd->bgqd",
        weights.astype(jnp.bfloat16),
        value_rows,
        preferred_element_type=jnp.float32,
    )
    run_max, run_sum, run_acc = combined_all((local_max, local_sum, local_acc), "kv", combine_parts)
    own_score = (
        jnp.einsum("bgqd,bgd->bgq", query, key_new, preferred_element_type=jnp.float32)
        * score_scale
    )
    larger = jnp.maximum(run_max, own_score)
    keep_factor = jnp.exp(run_max - larger)
    own_weight = jnp.exp(own_score - larger)
    total = run_sum * keep_factor + own_weight
    attended = (
        run_acc * keep_factor[..., None]
        + own_weight[..., None] * value_new.astype(jnp.float32)[:, :, None, :]
    ) / total[..., None]
    attended = attended.astype(jnp.bfloat16).reshape(batch_rows, kv_here * group_size * HD)
    out_part = jnp.dot(attended, w_output, preferred_element_type=jnp.float32)
    out_sum = lax.psum_scatter(
        out_part.astype(jnp.bfloat16), "tp", scatter_dimension=1, tiled=True
    ).astype(jnp.float32)
    residual_mine = hidden_in.astype(jnp.float32) + out_sum
    mid_block = lax.all_gather(residual_mine, "tp", axis=1, tiled=True)
    mid_scaled = (mid_block * mid_gain).astype(jnp.bfloat16)
    mid_square = jnp.sum(mid_block * mid_block, axis=1, keepdims=True)
    gate_part = jnp.dot(mid_scaled, w_gate, preferred_element_type=jnp.float32)
    up_part = jnp.dot(mid_scaled, w_up, preferred_element_type=jnp.float32)
    gate_sum, up_sum, mid_total = lax.psum((gate_part, up_part, mid_square), "kv")
    mid_inv = lax.rsqrt(mid_total / D + norm_eps)
    hidden_units = (jax.nn.silu(gate_sum * mid_inv) * (up_sum * mid_inv)).astype(jnp.bfloat16)
    down_part = jnp.dot(hidden_units, w_down, preferred_element_type=jnp.float32)
    down_sum = lax.psum_scatter(
        down_part.astype(jnp.bfloat16), "tp", scatter_dimension=1, tiled=True
    ).astype(jnp.float32)
    return residual_mine + down_sum


def solution(mesh):
    in_specs = (
        P(None, ("kv", "tp")),
        P("kv"),
        P("kv", "tp"),
        P("kv", "tp"),
        P("kv", "tp"),
        P("kv", None),
        P("tp"),
        P(None, "kv", "tp"),
        P(None, "kv", "tp"),
        P(None, "tp", "kv"),
        P("tp", "kv"),
        P("kv"),
        P("kv", "tp"),
        P("kv", "tp"),
        P("tp", "kv"),
    )
    out_specs = P(None, ("kv", "tp"))
    return jax.shard_map(
        on_device, mesh=mesh, in_specs=in_specs, out_specs=out_specs, check_vma=False
    )
```

profile of v0, /device:TPU:0, one launch (start us, length us, event | category | flops | bytes accessed | tf_op | source)
XLA Modules:
  0.0 351.1 jit_solution(4639241482038854602)
XLA Ops:
  6.5 6.5 %all_gather.24 = bf16[16,512]{1,0:T(8,128)(2,1)S(1)} all-gather(bf16[16,128]{1,0:T(8,128)(2,1)} %param.17), channel_id=1, replica_groups=mesh['kv'=8,'tp'=4] {'tp'}, dimensions={1}, use_global_device_ids=true | all-gather | bytes 20480 | tf_op jit(solution)/shard_map/all_gather | solution.py:69
  13.0 0.7 fusion.15
  13.7 2.0 fusion.23
  15.7 1.7 fusion.17
  17.4 1.7 fusion.19
  19.2 1.5 fusion.21
  20.7 12.3 %copy.38 = bf16[16,1024,256]{1,2,0:T(8,128)(2,1)} copy(bf16[16,1024,256]{2,1,0:T(8,128)(2,1)} %param.24) | data formatting | bytes 16777216 | tf_op args[7]
  33.0 12.4 %copy.40 = bf16[16,1024,256]{1,2,0:T(8,128)(2,1)} copy(bf16[16,1024,256]{2,1,0:T(8,128)(2,1)} %param.25) | data formatting | bytes 16777216 | tf_op args[8]
  45.4 48.6 %all-reduce.5.cloned.1.call-done = (f32[16,768]{1,0:T(8,128)}, f32[16,1]{0,1:T(1,128)}, f32[16,16]{0,1:T(8,128)}, f32[16,256]{1,0:T(8,128)}, f32[16,256]{1,0:T(8,128)}) async-done(((f32[16,768]{1,0:T(8,128)}, f32[16,1]{0,1:T(1,128)}, f32[16,16]{0,1:T(8,128)}, f32[16,256]{1,0:T(8,128)}, f32[16,256]{1,0:T(8,128)}), (f32[16,768]{1,0:T(8,128)}, f32[16,1]{0,1:T(1,128)}, f32[16,16]{0,1:T(8,128)}, ...) | async-done | bytes 83024 | tf_op jit(solution)/shard_map/psum | solution.py:73
  94.0 0.7 rsqrt_bitcast_fusion.1
  94.7 0.8 fusion.29
  95.5 0.9 multiply_convert_fusion.2
  96.5 4.8 %fusion.36 = (f32[16,4,3]{2,1,0:T(4,128)S(1)}, f32[16,4,3,1024]{3,2,1,0:T(4,128)S(1)}) fusion(f32[16,4,1024]{2,1,0:T(4,128)S(1)} %copy-done.4, f32[16,4]{1,0:T(8,128)S(1)} %copy.39, bf16[16,4,3,64]{3,2,1,0:T(4,128)(2,1)S(1)} %reshape.34, bf16[16,1024,4,64]{1,3,2,0:T(8,128)(2,1)} %bitcast.58), kind=kOutput, calls=%fused_computation.57 | convolution fusion | flops 25952064 | bytes 9462784 | tf_op jit(solution)/shard_map/bgqd,bpgd->bgqp/dot_general | solution.py:86
  101.4 30.8 %all-gather = f32[128,4,3]{2,1,0:T(4,128)S(1)} all-gather(f32[16,4,3]{2,1,0:T(4,128)S(1)} %get-tuple-element.230), channel_id=2, replica_groups=mesh['kv'=8,'tp'=4] {'kv'}, dimensions={0}, use_global_device_ids=true | all-gather | bytes 6912 | tf_op jit(solution)/shard_map/all_gather | solution.py:16
  132.7 2.3 fusion.8
  135.1 32.1 %all-gather.2 = f32[128,4,3,64]{3,1,2,0:T(4,128)S(1)} all-gather(f32[16,4,3,64]{3,1,2,0:T(4,128)S(1)} %copy.41), channel_id=4, replica_groups=mesh['kv'=8,'tp'=4] {'kv'}, dimensions={0}, use_global_device_ids=true | all-gather | bytes 442368 | tf_op jit(solution)/shard_map/all_gather | solution.py:16
  167.2 0.9 copy-done.3
  168.2 30.7 %all-gather.1 = f32[128,4,3]{2,1,0:T(4,128)S(1)} all-gather(f32[16,4,3]{2,1,0:T(4,128)S(1)} %fusion.7), channel_id=3, replica_groups=mesh['kv'=8,'tp'=4] {'kv'}, dimensions={0}, use_global_device_ids=true | all-gather | bytes 6912 | tf_op jit(solution)/shard_map/all_gather | solution.py:16
  199.5 0.9 copy.48
  200.4 0.9 copy.45
  201.7 16.0 %while.19 = (s32[]{:T(128)}, f32[16,4,3]{0,1,2:T(4,128)S(1)}, f32[16,4,3]{0,1,2:T(4,128)S(1)}, f32[16,4,3,64]{3,2,1,0:T(4,128)S(1)}, f32[8,16,4,3]{1,2,3,0:T(4,1...) while((s32[]{:T(128)}, f32[16,4,3]{0,1,2:T(4,128)S(1)}, ...), condition=%wide.region_7.8_spmd, body=%wide.region_6.7_spmd.sunk | while | flops 38021 | bytes 256663 | solution.py:21
  201.7 0.7 fusion.54
  202.6 0.9 constant_dynamic-slice_fusion.2
  204.0 0.7 fusion.54
  204.9 0.9 constant_dynamic-slice_fusion.2
  206.3 0.7 fusion.54
  207.2 0.9 constant_dynamic-slice_fusion.2
  208.6 0.7 fusion.54
  209.5 0.9 constant_dynamic-slice_fusion.2
  210.9 0.7 fusion.54
  211.8 0.9 constant_dynamic-slice_fusion.2
  213.1 0.7 fusion.54
  214.1 0.9 constant_dynamic-slice_fusion.2
  215.4 0.7 fusion.54
  216.4 0.9 constant_dynamic-slice_fusion.2
  219.0 1.4 convolution_convert_fusion.1
  220.4 0.8 copy.59
  221.2 19.1 %reduce-scatter.7.cloned.1.call-done = bf16[128,16]{1,0:T(8,128)(2,1)} async-done(((bf16[512,16]{1,0:T(8,128)(2,1)}), bf16[128,16]{1,0:T(8,128)(2,1)}) %reduce-scatter.7.cloned.1.call-update) | async-done | bytes 4112
  240.3 0.8 copy.60
  241.1 5.3 %all_gather.31 = f32[16,512]{1,0:T(8,128)S(1)} all-gather(f32[16,128]{1,0:T(8,128)S(1)} %convert_add_fusion.1), channel_id=1, replica_groups=mesh['kv'=8,'tp'=4] {'tp'}, dimensions={1}, use_global_device_ids=true | all-gather | bytes 40960 | tf_op jit(solution)/shard_map/all_gather | solution.py:118
  246.5 1.2 fusion.27
  247.6 1.2 fusion.28
  249.0 21.5 %psum.62 = f32[16,1]{0,1:T(1,128)S(1)} all-reduce(f32[16,1]{0,1:T(1,128)S(1)} %bitcast.68), channel_id=1, replica_groups=mesh['kv'=8,'tp'=4] {'kv'}, use_global_device_ids=true, to_apply=%region_13.14 | all-reduce | flops 16 | bytes 128 | tf_op jit(solution)/shard_map/psum | solution.py:123
  270.4 50.3 %all-reduce.7.cloned.1.call-done = (f32[16,2816]{1,0:T(8,128)}, f32[16,2816]{1,0:T(8,128)}) async-done(((f32[16,2816]{1,0:T(8,128)}, f32[16,2816]{1,0:T(8,128)}), (f32[16,2816]{1,0:T(8,128)}, f32[16,2816]{1,0:T(8,128)})) %all-reduce.7.cloned.1.call-update) | async-done | bytes 360464 | tf_op jit(solution)/shard_map/psum | solution.py:123
  320.7 2.6 convolution_convert_fusion
  323.3 0.8 copy.61
  324.0 19.1 %reduce-scatter.9.cloned.1.call-done = bf16[128,16]{1,0:T(8,128)(2,1)} async-done(((bf16[512,16]{1,0:T(8,128)(2,1)}), bf16[128,16]{1,0:T(8,128)(2,1)}) %reduce-scatter.9.cloned.1.call-update) | async-done | bytes 4112
  343.1 0.8 copy.62
  (81 shorter events, 8.6 us)
Async XLA Ops:
  6.5 239.9 %copy-start = (bf16[512,2816]{1,0:T(8,128)(2,1)S(1)}, bf16[512,2816]{1,0:T(8,128)(2,1)}, u32[]{:S(2)}) copy-start(bf16[512,2816]{1,0:T(8,128)(2,1)} %param.30) | copy-start | bytes 8650756
  6.5 87.4 %all-reduce.5.cloned.1.call-start = ((), (), s32[]{:S(2)}) async-start(), calls=%async_computation.4 | async-start | bytes 181248 | tf_op jit(solution)/shard_map/psum | solution.py:73
  20.6 219.7 %reduce-scatter.7.cloned.1.call-start = ((), (), s32[]{:S(2)}) async-start(), calls=%async_computation.2 | async-start | bytes 163840
  33.0 61.6 %copy-start.13 = (f32[4]{0:T(128)S(1)}, f32[4]{0:T(128)}, u32[]{:S(2)}) copy-start(f32[4]{0:T(128)} %param.23) | copy-start | bytes 52
  33.0 63.5 %copy-start.4 = (f32[16,4,1024]{2,1,0:T(4,128)S(1)}, f32[16,4,1024]{2,1,0:T(4,128)}, u32[]{:S(2)}) copy-start(f32[16,4,1024]{2,1,0:T(4,128)} %param.26) | copy-start | bytes 786436
  94.6 0.9 copy-start.11
  96.5 4.9 %copy-start.5 = (bf16[16,4,3,64]{3,2,1,0:T(4,128)(2,1)}, bf16[16,4,3,64]{3,2,1,0:T(4,128)(2,1)S(1)}, u32[]{:S(2)}) copy-start(bf16[16,4,3,64]{3,2,1,0:T(4,128)(2,1)S(1)} %reshape.34) | copy-start | bytes 73732
  96.5 36.2 %copy-start.1 = (bf16[16,1024,256]{1,2,0:T(8,128)(2,1)S(1)}, bf16[16,1024,256]{1,2,0:T(8,128)(2,1)}, u32[]{:S(2)}) copy-start(bf16[16,1024,256]{1,2,0:T(8,128)(2,1)} %copy.40) | copy-start | bytes 25165828
  167.2 0.9 copy-start.3
  168.1 49.6 %copy-start.8 = (f32[16,256]{1,0:T(8,128)S(1)}, f32[16,256]{1,0:T(8,128)}, u32[]{:S(2)}) copy-start(f32[16,256]{1,0:T(8,128)} %get-tuple-element.217) | copy-start | bytes 49156
  200.4 17.3 %copy-start.9 = (f32[16,256]{1,0:T(8,128)S(1)}, f32[16,256]{1,0:T(8,128)}, u32[]{:S(2)}) copy-start(f32[16,256]{1,0:T(8,128)} %get-tuple-element.218) | copy-start | bytes 49156
  200.4 17.3 %copy-start.12 = (f32[16]{0:T(128)S(1)}, f32[16]{0:T(128)}, u32[]{:S(2)}) copy-start(f32[16]{0:T(128)} %copy-done.11) | copy-start | bytes 196
  200.4 17.5 %copy-start.6 = (bf16[16,4,3,64]{3,2,1,0:T(4,128)(2,1)S(1)}, bf16[16,4,3,64]{3,2,1,0:T(4,128)(2,1)}, u32[]{:S(2)}) copy-start(bf16[16,4,3,64]{3,2,1,0:T(4,128)(2,1)} %copy-done.5) | copy-start | bytes 73732
  201.7 39.4 %copy-start.7 = (bf16[16,128]{1,0:T(8,128)(2,1)S(1)}, bf16[16,128]{1,0:T(8,128)(2,1)}, u32[]{:S(2)}) copy-start(bf16[16,128]{1,0:T(8,128)(2,1)} %param.17) | copy-start | bytes 12292
  201.7 44.8 %copy-start.10 = (f32[512]{0:T(512)S(1)}, f32[512]{0:T(512)}, u32[]{:S(2)}) copy-start(f32[512]{0:T(512)} %param.28) | copy-start | bytes 6148
  221.2 99.5 %all-reduce.7.cloned.1.call-start = ((), (), s32[]{:S(2)}) async-start(), calls=%async_computation.5 | async-start | bytes 720896 | tf_op jit(solution)/shard_map/psum | solution.py:123
  241.1 6.5 %copy-start.2 = (bf16[512,2816]{1,0:T(8,128)(2,1)S(1)}, bf16[512,2816]{1,0:T(8,128)(2,1)}, u32[]{:S(2)}) copy-start(bf16[512,2816]{1,0:T(8,128)(2,1)} %param.29) | copy-start | bytes 8650756
  248.8 94.3 %reduce-scatter.9.cloned.1.call-start = ((), (), s32[]{:S(2)}) async-start(), calls=%async_computation.3 | async-start | bytes 163840
Sparse Core Ops, SparseCore 0:
  20.8 73.1 all-reduce.4
  221.3 18.9 reduce-scatter.6
  248.9 71.7 all-reduce.6
  324.2 18.9 reduce-scatter.8
where the time goes:
time: 353 us; the launch traced here: 351 us
  waiting for transfers between devices  137 us (39%)
  blocking collectives  127 us (36%)
  local copies, waits for them, and re-layouts  40.4 us (11%)
  matrix products  20.5 us (6%)
  between operations  13.3 us (4%)
  other arithmetic  12.7 us (4%)
    all_gather x3, blocking collectives, combined_all(): gathered = jax.tree.map(lambda a: lax.all_gather(a, axis), part)  93.7 us
    psum x1, waiting for transfers between devices, on_device(): lax.psum((gate_part, up_part, mid_square), 'kv')  50.3 us
    psum x1, waiting for transfers between devices, on_device(): lax.psum((q_part, k_part, v_part, f_part, square), 'kv')  48.6 us
    unnamed x6, waiting for transfers between devices  38.2 us
    unnamed x34, local copies, waits for them, and re-layouts  28.8 us
    psum x1, blocking collectives, on_device(): lax.psum((gate_part, up_part, mid_square), 'kv')  21.5 us
  transfers between devices with their start and end apart: 4, of which 4 were waited for; matrix products, arithmetic and copies ran while one was open for 7% of the time, Pallas kernels for 0%

commit v1 on v0

v1 whole, which is shorter than its diff:
```python
import functools

import jax
import jax.numpy as jnp
from jax import lax
from jax.experimental import pallas as pl
from jax.experimental.pallas import tpu as pltpu
from jax.sharding import PartitionSpec as P

HD = 64
norm_eps = 1e-06
F32 = jnp.float32
BF16 = jnp.bfloat16
MESH = pl.DeviceIdType.MESH


def exchange(axis, n, me, send_sem, recv_sem, source_of, target_of):
    copies = []
    for k in range(1, n):
        peer = lax.rem(me + k, n)
        copy = pltpu.make_async_remote_copy(
            src_ref=source_of(peer),
            dst_ref=target_of(k),
            send_sem=send_sem.at[k],
            recv_sem=recv_sem.at[k],
            device_id={axis: peer},
            device_id_type=MESH,
        )
        copy.start()
        copies.append(copy)
    return copies


def layer_kernel(
    n_kv, n_tp, group, d_model,
    hid_ref, pg_ref, wf_ref, mg_ref, bias_ref,
    wq_hbm, wk_hbm, wv_hbm, kc_hbm, vc_hbm, dec_hbm, wo_hbm, wg_hbm, wu_hbm, wd_hbm,
    out_ref,
    wq, wk, wv, kc, vc, dec, wo, wg, wu, wd,
    hbuf, pbuf, prec, qbuf, qm, qbd, fold, cbuf, crec, abuf, orec, gbuf, grec, ubuf, dbuf, drec, mine,
    load_sem, wo_sem, kv_send, kv_recv, tp_send, tp_recv,
):
    mk = lax.axis_index("kv")
    mt = lax.axis_index("tp")
    batch = hid_ref.shape[0]
    lanes = hid_ref.shape[1]
    nb = batch // n_kv
    nq, nk, ff = wq.shape[1], wk.shape[1], wg.shape[1]
    kvh = nk // HD
    span = group + 1
    rows = qbd.shape[1]
    positions = kc.shape[1]

    pairs = ((wq_hbm, wq), (wk_hbm, wk), (wv_hbm, wv), (kc_hbm, kc), (dec_hbm, dec), (vc_hbm, vc),
             (wg_hbm, wg), (wu_hbm, wu), (wd_hbm, wd))
    loads = [pltpu.make_async_copy(a, b, load_sem.at[i]) for i, (a, b) in enumerate(pairs)]
    ld_q, ld_k, ld_v, ld_kc, ld_dec, ld_vc, ld_g, ld_u, ld_d = loads
    wo_loads = []
    for g in range(kvh):
        for j in range(group):
            wo_loads.append(pltpu.make_async_copy(
                wo_hbm.at[pl.ds((g * group + j) * HD, HD)],
                wo.at[pl.ds(j * nk + g * HD, HD)],
                wo_sem.at[g * group + j]))
    for c in (ld_q, ld_k, ld_v, ld_kc, ld_dec, ld_vc):
        c.start()
    for c in wo_loads:
        c.start()
    for c in (ld_g, ld_u, ld_d):
        c.start()

    barrier = pltpu.get_barrier_semaphore()
    for k in range(1, n_tp):
        pl.semaphore_signal(barrier, inc=1, device_id={"tp": lax.rem(mt + k, n_tp)}, device_id_type=MESH)
    for k in range(1, n_kv):
        pl.semaphore_signal(barrier, inc=1, device_id={"kv": lax.rem(mk + k, n_kv)}, device_id_type=MESH)
    pl.semaphore_wait(barrier, n_tp + n_kv - 2)

    pending = []
    c_h = exchange("tp", n_tp, mt, tp_send.at[0], tp_recv.at[0], lambda peer: hid_ref, lambda k: hbuf.at[mt])
    pending += c_h
    hbuf[mt] = hid_ref[...]

    col = lax.broadcasted_iota(jnp.int32, (nq, nk), 0)
    col2 = lax.broadcasted_iota(jnp.int32, (nq, nk), 1)
    head_col = sum(((col >= t * group * HD).astype(jnp.int32) for t in range(1, kvh)), jnp.zeros_like(col))
    same = ((col & (HD - 1)) == (col2 & (HD - 1))) & (head_col == lax.shift_right_logical(col2, 6))
    fold[...] = jnp.where(same, HD ** (-0.5), 0.0).astype(BF16)
    mcol = lax.broadcasted_iota(jnp.int32, (rows, nq), 1)
    mrow = lax.broadcasted_iota(jnp.int32, (rows, nq), 0)
    mhead = sum(((mcol >= t * group * HD).astype(jnp.int32) for t in range(1, kvh)), jnp.zeros_like(mcol))
    mask = (mhead * span + lax.shift_right_logical(mcol, 6) - mhead * group) == mrow
    group_of_col = lax.shift_right_logical(lax.broadcasted_iota(jnp.int32, (span, nk), 1), 6)
    span_row = lax.broadcasted_iota(jnp.int32, (span, nk), 0)
    lane_i = lax.broadcasted_iota(jnp.int32, (rows, nk), 1)
    row_i = lax.broadcasted_iota(jnp.int32, (rows, nk), 0)
    eye_max = lane_i == row_i
    eye_sum = lane_i == row_i + rows
    row_one = lax.broadcasted_iota(jnp.int32, (rows, 1), 0)
    row_group = sum(((row_one >= t * span).astype(jnp.int32) for t in range(1, kvh)), jnp.zeros_like(row_one))
    frow = lax.broadcasted_iota(jnp.int32, (rows, 128), 0)
    fgroup = sum(((frow >= t * span).astype(jnp.int32) for t in range(1, kvh)), jnp.zeros_like(frow))
    pick_forget = lax.broadcasted_iota(jnp.int32, (rows, 128), 1) == fgroup + mt * kvh
    bias = jnp.zeros((rows, 1), F32)
    for g in range(kvh):
        bias = jnp.where(row_group == g, bias_ref[g], bias)

    def collapse(x):
        total = jnp.zeros((span, nk), F32)
        for g in range(kvh):
            total = jnp.where(group_of_col == g, x[g * span:(g + 1) * span], total)
        return total

    for c in c_h:
        c.wait_recv()
    block = jnp.concatenate([hbuf[t] for t in range(n_tp)], axis=1).astype(F32)
    scaled = (block * pg_ref[...]).astype(BF16)
    square = jnp.sum(block * block, axis=1, keepdims=True)
    f_part = jnp.dot(scaled, wf_ref[...], preferred_element_type=F32)
    nf = f_part.shape[1]
    base = nq + 2 * nk
    pbuf[:, :, base:base + nf] = f_part.reshape(batch, 1, nf)
    pbuf[:, :, base + nf:] = jnp.broadcast_to(square, (batch, 128 - nf)).reshape(batch, 1, 128 - nf)
    ld_q.wait()
    pbuf[:, :, 0:nq] = jnp.dot(scaled, wq[...], preferred_element_type=F32).reshape(batch, 1, nq)
    ld_k.wait()
    pbuf[:, :, nq:nq + nk] = jnp.dot(scaled, wk[...], preferred_element_type=F32).reshape(batch, 1, nk)
    ld_v.wait()
    pbuf[:, :, nq + nk:base] = jnp.dot(scaled, wv[...], preferred_element_type=F32).reshape(batch, 1, nk)
    c_p = exchange("kv", n_kv, mk, kv_send.at[0], kv_recv.at[0],
                   lambda peer: pbuf.at[pl.ds(peer * nb, nb)], lambda k: prec.at[k])
    pending += c_p
    for c in c_p:
        c.wait_recv()
    keys_own, values_own, logs_own = [], [], []
    for i in range(nb):
        total = pbuf[mk * nb + i]
        for k in range(1, n_kv):
            total = total + prec[k, i]
        inv = lax.rsqrt(total[:, base + 127:base + 128] / d_model + norm_eps)
        qbuf[mk * nb + i] = (total[:, 0:nq] * inv).astype(BF16).astype(F32)
        keys_own.append((total[:, nq:nq + nk] * inv).astype(BF16).astype(F32))
        values_own.append((total[:, nq + nk:base] * inv).astype(BF16).astype(F32))
        forget = jnp.broadcast_to(total[:, base:base + 128] * inv, (rows, 128))
        forget = jnp.sum(jnp.where(pick_forget, forget, 0.0), axis=1, keepdims=True) + bias
        logs_own.append(jnp.minimum(forget, 0.0) - jnp.log(1.0 + jnp.exp(-jnp.abs(forget))))
    own_rows = pl.ds(mk * nb, nb)
    c_q = exchange("kv", n_kv, mk, kv_send.at[1], kv_recv.at[1],
                   lambda peer: qbuf.at[own_rows], lambda k: qbuf.at[own_rows])
    pending += c_q
    for c in c_q:
        c.wait_recv()
    for b in range(batch):
        qm[b * rows:(b + 1) * rows, :] = jnp.where(mask, jnp.broadcast_to(qbuf[b], (rows, nq)), 0.0).astype(BF16)
    qbd[...] = jnp.dot(qm[...], fold[...], preferred_element_type=F32).astype(BF16).reshape(batch, rows, nk)

    ld_kc.wait()
    ld_dec.wait()
    ld_vc.wait()

    def attend(b, carry):
        scores = lax.dot_general(qbd[b], kc[b], (((1,), (1,)), ((), ())), preferred_element_type=F32)
        decay = dec[b]
        parts = [jnp.broadcast_to(decay[g:g + 1], (span, positions)) for g in range(kvh)]
        if rows > kvh * span:
            parts.append(jnp.broadcast_to(decay[0:1], (rows - kvh * span, positions)))
        scores = scores + jnp.concatenate(parts, axis=0)
        top = jnp.max(scores, axis=1, keepdims=True)
        weights = jnp.exp(scores - top)
        total = jnp.sum(weights, axis=1, keepdims=True)
        acc = jnp.dot(weights.astype(BF16), vc[b], preferred_element_type=F32)
        stat = jnp.sum(jnp.where(eye_max, top, jnp.where(eye_sum, total, 0.0)), axis=0, keepdims=True)
        cbuf[b] = jnp.where(span_row == group, jnp.broadcast_to(stat, (span, nk)), collapse(acc))
        return carry

    lax.fori_loop(0, batch, attend, 0, unroll=4)

    c_c = exchange("kv", n_kv, mk, kv_send.at[2], kv_recv.at[2],
                   lambda peer: cbuf.at[pl.ds(peer * nb, nb)], lambda k: crec.at[k])
    pending += c_c
    for c in c_c:
        c.wait_recv()
    for i in range(nb):
        messages = [cbuf[mk * nb + i]] + [crec[k, i] for k in range(1, n_kv)]
        tops, totals = [], []
        for message in messages:
            stat = jnp.broadcast_to(message[group:group + 1], (rows, nk))
            tops.append(jnp.sum(jnp.where(eye_max, stat, 0.0), axis=1, keepdims=True) + logs_own[i])
            totals.append(jnp.sum(jnp.where(eye_sum, stat, 0.0), axis=1, keepdims=True))
        own = jnp.sum(qbd[mk * nb + i].astype(F32) * keys_own[i], axis=1, keepdims=True)
        top = functools.reduce(jnp.maximum, tops, own)
        own_weight = jnp.exp(own - top)
        factors = [jnp.exp(t - top) for t in tops]
        norm = own_weight
        for factor, total in zip(factors, totals):
            norm = norm + factor * total
        attended = collapse(jnp.broadcast_to(own_weight / norm, (rows, nk))) * values_own[i]
        for factor, message in zip(factors, messages):
            attended = attended + message * collapse(jnp.broadcast_to(factor / norm, (rows, nk)))
        attended = jnp.where(span_row == group, 0.0, attended)
        abuf[mk * nb + i] = attended.astype(BF16).astype(F32)
    c_a = exchange("kv", n_kv, mk, kv_send.at[3], kv_recv.at[3],
                   lambda peer: abuf.at[own_rows], lambda k: abuf.at[own_rows])
    pending += c_a
    for c in wo_loads:
        c.wait()
    for c in c_a:
        c.wait_recv()
    out_part = jnp.zeros((batch, wo.shape[1]), F32)
    for j in range(group):
        out_part = out_part + jnp.dot(
            abuf[:, j, :].astype(BF16), wo[j * nk:(j + 1) * nk, :], preferred_element_type=F32)
    orec[mt] = out_part.astype(BF16)
    c_o = exchange("tp", n_tp, mt, tp_send.at[1], tp_recv.at[1], lambda peer: orec.at[mt], lambda k: orec.at[mt])
    pending += c_o
    for c in c_o:
        c.wait_recv()
    projected = orec[0].astype(F32)
    for t in range(1, n_tp):
        projected = projected + orec[t].astype(F32)
    after = block + projected
    for t in range(n_tp):
        mine[t] = after[:, t * lanes:(t + 1) * lanes]
    mid = (after * mg_ref[...]).astype(BF16)
    mid_square = jnp.sum(after * after, axis=1, keepdims=True)
    ld_g.wait()
    gbuf[:, :, 0:ff] = jnp.dot(mid, wg[...], preferred_element_type=F32).reshape(batch, 1, ff)
    ld_u.wait()
    gbuf[:, :, ff:2 * ff] = jnp.dot(mid, wu[...], preferred_element_type=F32).reshape(batch, 1, ff)
    gbuf[:, :, 2 * ff:] = jnp.broadcast_to(mid_square, (batch, 128)).reshape(batch, 1, 128)
    c_g = exchange("kv", n_kv, mk, kv_send.at[4], kv_recv.at[4],
                   lambda peer: gbuf.at[pl.ds(peer * nb, nb)], lambda k: grec.at[k])
    pending += c_g
    for c in c_g:
        c.wait_recv()
    for i in range(nb):
        total = gbuf[mk * nb + i]
        for k in range(1, n_kv):
            total = total + grec[k, i]
        inv = lax.rsqrt(total[:, 2 * ff:2 * ff + 1] / d_model + norm_eps)
        gate = total[:, 0:ff] * inv
        up = total[:, ff:2 * ff] * inv
        ubuf[mk * nb + i] = gate / (1.0 + jnp.exp(-gate)) * up
    c_u = exchange("kv", n_kv, mk, kv_send.at[5], kv_recv.at[5],
                   lambda peer: ubuf.at[own_rows], lambda k: ubuf.at[own_rows])
    pending += c_u
    ld_d.wait()
    for c in c_u:
        c.wait_recv()
    units = ubuf[:, 0, :].astype(BF16)
    down = jnp.dot(units, wd[...], preferred_element_type=F32).astype(BF16)
    for t in range(n_tp):
        dbuf[t] = down[:, t * lanes:(t + 1) * lanes]
    c_d = exchange("tp", n_tp, mt, tp_send.at[2], tp_recv.at[2], lambda peer: dbuf.at[peer], lambda k: drec.at[k])
    pending += c_d
    for c in c_d:
        c.wait_recv()
    lowered = dbuf[mt].astype(F32)
    for k in range(1, n_tp):
        lowered = lowered + drec[k].astype(F32)
    out_ref[...] = mine[mt] + lowered
    for c in pending:
        c.wait_send()


def on_device(
    n_kv, n_tp,
    hidden_in, pre_gain, w_query, w_key, w_value, w_forget, forget_bias, key_cache, value_cache,
    decay_to_end, w_output, mid_gain, w_gate, w_up, w_down,
):
    batch, lanes = hidden_in.shape
    depth, nq = w_query.shape
    nk = w_key.shape[1]
    ff = w_gate.shape[1]
    kvh = decay_to_end.shape[1]
    group = nq // nk
    d_model = lanes * n_kv * n_tp
    span = group + 1
    rows = max(16, -(-kvh * span // 16) * 16)
    nb = batch // n_kv
    width = nq + 2 * nk + 128
    wide = 2 * ff + 128
    vmem = pl.BlockSpec(memory_space=pltpu.VMEM)
    anywhere = pl.BlockSpec(memory_space=pl.ANY)
    big = (w_query, w_key, w_value, key_cache, value_cache, decay_to_end, w_output, w_gate, w_up, w_down)
    scratch = [pltpu.VMEM(a.shape, a.dtype) for a in big] + [
        pltpu.VMEM((n_tp, batch, lanes), BF16),
        pltpu.VMEM((batch, 1, width), F32),
        pltpu.VMEM((n_kv, nb, 1, width), F32),
        pltpu.VMEM((batch, 1, nq), F32),
        pltpu.VMEM((batch * rows, nq), BF16),
        pltpu.VMEM((batch, rows, nk), BF16),
        pltpu.VMEM((nq, nk), BF16),
        pltpu.VMEM((batch, span, nk), F32),
        pltpu.VMEM((n_kv, nb, span, nk), F32),
        pltpu.VMEM((batch, span, nk), F32),
        pltpu.VMEM((n_tp, batch, w_output.shape[1]), BF16),
        pltpu.VMEM((batch, 1, wide), F32),
        pltpu.VMEM((n_kv, nb, 1, wide), F32),
        pltpu.VMEM((batch, 1, ff), F32),
        pltpu.VMEM((n_tp, batch, lanes), BF16),
        pltpu.VMEM((n_tp, batch, lanes), BF16),
        pltpu.VMEM((n_tp, batch, lanes), F32),
        pltpu.SemaphoreType.DMA((9,)),
        pltpu.SemaphoreType.DMA((kvh * group,)),
        pltpu.SemaphoreType.DMA((6, n_kv)),
        pltpu.SemaphoreType.DMA((6, n_kv)),
        pltpu.SemaphoreType.DMA((3, n_tp)),
        pltpu.SemaphoreType.DMA((3, n_tp)),
    ]
    return pl.pallas_call(
        functools.partial(layer_kernel, n_kv, n_tp, group, d_model),
        out_shape=jax.ShapeDtypeStruct((batch, lanes), F32),
        in_specs=[vmem] * 4 + [pl.BlockSpec(memory_space=pltpu.SMEM)] + [anywhere] * 10,
        out_specs=vmem,
        scratch_shapes=scratch,
        compiler_params=pltpu.CompilerParams(
            collective_id=0, has_side_effects=True, vmem_limit_bytes=60 * 1024 * 1024
        ),
        name="decode_layer",
    )(hidden_in, pre_gain.reshape(1, -1), w_forget, mid_gain.reshape(1, -1), forget_bias, *big)


def solution(mesh):
    in_specs = (
        P(None, ("kv", "tp")),
        P("kv"),
        P("kv", "tp"),
        P("kv", "tp"),
        P("kv", "tp"),
        P("kv", None),
        P("tp"),
        P(None, "kv", "tp"),
        P(None, "kv", "tp"),
        P(None, "tp", "kv"),
        P("tp", "kv"),
        P("kv"),
        P("kv", "tp"),
        P("kv", "tp"),
        P("tp", "kv"),
    )
    return jax.shard_map(
        functools.partial(on_device, mesh.shape["kv"], mesh.shape["tp"]),
        mesh=mesh,
        in_specs=in_specs,
        out_specs=P(None, ("kv", "tp")),
        check_vma=False,
    )
```

time: 353 us -> 63.2 us (0.18)
  waiting for transfers between devices: 137 us -> 0 us
  blocking collectives: 127 us -> 0 us
  Pallas kernels: 0 us -> 60.1 us
  local copies, waits for them, and re-layouts: 40.4 us -> 2.75 us
  matrix products: 20.5 us -> 0 us
  between operations: 13.3 us -> 0.01 us
  other arithmetic: 12.7 us -> 0 us
    all_gather x5 -> x0, blocking collectives: 106 us -> none  [the longest x3 93.7 us: combined_all(): gathered = jax.tree.map(lambda a: lax.all_gather(a, axis), part)]
    psum x2 -> x0, waiting for transfers between devices: 98.8 us -> none  [the longest x1 50.3 us: on_device(): lax.psum((gate_part, up_part, mid_square), 'kv')]
    pallas_call x0 -> x1, Pallas kernels: none -> 60.1 us  [on_device(): pl.pallas_call(functools.partial(layer_kernel, n_kv, n_tp, group, d_model...]
    unnamed x6 -> x0, waiting for transfers between devices: 38.2 us -> none
    unnamed x34 -> x2, local copies, waits for them, and re-layouts: 28.8 us -> 2.75 us
    psum x1 -> x0, blocking collectives: 21.5 us -> none  [on_device(): lax.psum((gate_part, up_part, mid_square), 'kv')]
    dot_general x11 -> x0, matrix products: 20.5 us -> none  [the longest x1 4.82 us: on_device(): jnp.einsum('bgqd,bpgd->bgqp', query, key_rows, preferred_element_type=jnp...]
    add x17 -> x0, other arithmetic: 8.72 us -> none  [the longest x7 5.06 us: combine_parts(): sum_first * scale_first + sum_second * scale_second]
  transfers between devices with their start and end apart: 4 -> 0, of which waited for: 4 -> 0; matrix products, arithmetic and copies ran while one was open for 7% -> 0% of each run, Pallas kernels for 0% -> 0%
where the time goes in v1:
time: 63.2 us; the launch traced here: 62.9 us
  Pallas kernels  60.1 us (95%)
  local copies, waits for them, and re-layouts  2.75 us (4%)
    pallas_call x1, Pallas kernels, on_device(): pl.pallas_call(functools.partial(layer_kernel, n_kv, n_tp, group, d_model...  60.1 us
    unnamed x2, local copies, waits for them, and re-layouts  2.75 us

profile of v1, /device:TPU:0, one launch (start us, length us, event | category | flops | bytes accessed | tf_op | source)
XLA Modules:
  0.0 62.9 jit_solution(10490776868187528527)
XLA Ops:
  0.0 1.5 %copy.16.wf_ref = bf16[512,16]{1,0:T(8,128)(2,1)} copy(bf16[512,16]{0,1:T(8,128)(2,1)} %param.20) | data formatting | bytes 32768 | tf_op args[5]
  1.5 60.1 %decode_layer.1 = f32[16,128]{1,0:T(8,128)} custom-call(bf16[16,128]{1,0:T(8,128)(2,1)} %hid_ref.1, f32[1,512]{1,0:T(1,128)} %bitcast.2, bf16[512,16]{1,0:T(8,128)(2,1)} %copy.16.wf_ref, f32[1,512]{1,0:T(1,128)} %bitcast.3, f32[4]{0:T(128)} %bias_ref.1, bf16[512,768]{1,0:T(8,128)(2,1)} %wq_hbm.1, bf16[512,256]{1,0:T(8,128)(2,1)} %wk_hbm.1, ...), custom_call_target="tpu_custom_call" | custom-call | tf_op jit(solution)/shard_map/decode_layer/pallas_call | solution.py:311
  61.6 1.3 %copy.18 = f32[16,128]{1,0:T(8,128)} copy(f32[16,128]{1,0:T(8,128)} %decode_layer.1) | data formatting | bytes 16384

commit v2 on v1

--- a/solution.py
+++ b/solution.py
@@ -14,7 +14,7 @@
 MESH = pl.DeviceIdType.MESH
 
 
-def exchange(axis, n, me, send_sem, recv_sem, source_of, target_of):
+def exchange(axis, n, me, send_sem, recv_sem, source_of, target_of, start=True):
     copies = []
     for k in range(1, n):
         peer = lax.rem(me + k, n)
@@ -26,7 +26,8 @@
             device_id={axis: peer},
             device_id_type=MESH,
         )
-        copy.start()
+        if start:
+            copy.start()
         copies.append(copy)
     return copies
 
@@ -37,7 +38,7 @@
     wq_hbm, wk_hbm, wv_hbm, kc_hbm, vc_hbm, dec_hbm, wo_hbm, wg_hbm, wu_hbm, wd_hbm,
     out_ref,
     wq, wk, wv, kc, vc, dec, wo, wg, wu, wd,
-    hbuf, pbuf, prec, qbuf, qm, qbd, fold, cbuf, crec, abuf, orec, gbuf, grec, ubuf, dbuf, drec, mine,
+    hbuf, pbuf, prec, qbuf, qm, qbd, fold, cbuf, crec, abuf, orec, gbuf, grec, ubuf, sq_own, srec, dbuf, drec, mine,
     load_sem, wo_sem, kv_send, kv_recv, tp_send, tp_recv,
 ):
     mk = lax.axis_index("kv")
@@ -116,7 +117,7 @@
     block = jnp.concatenate([hbuf[t] for t in range(n_tp)], axis=1).astype(F32)
     scaled = (block * pg_ref[...]).astype(BF16)
     square = jnp.sum(block * block, axis=1, keepdims=True)
-    f_part = jnp.dot(scaled, wf_ref[...], preferred_element_type=F32)
+    f_part = lax.dot_general(scaled, wf_ref[...], (((1,), (1,)), ((), ())), preferred_element_type=F32)
     nf = f_part.shape[1]
     base = nq + 2 * nk
     pbuf[:, :, base:base + nf] = f_part.reshape(batch, 1, nf)
@@ -158,7 +159,7 @@
     ld_dec.wait()
     ld_vc.wait()
 
-    def attend(b, carry):
+    def attend(b):
         scores = lax.dot_general(qbd[b], kc[b], (((1,), (1,)), ((), ())), preferred_element_type=F32)
         decay = dec[b]
         parts = [jnp.broadcast_to(decay[g:g + 1], (span, positions)) for g in range(kvh)]
@@ -171,12 +172,14 @@
         acc = jnp.dot(weights.astype(BF16), vc[b], preferred_element_type=F32)
         stat = jnp.sum(jnp.where(eye_max, top, jnp.where(eye_sum, total, 0.0)), axis=0, keepdims=True)
         cbuf[b] = jnp.where(span_row == group, jnp.broadcast_to(stat, (span, nk)), collapse(acc))
-        return carry
-
-    lax.fori_loop(0, batch, attend, 0, unroll=4)
 
     c_c = exchange("kv", n_kv, mk, kv_send.at[2], kv_recv.at[2],
-                   lambda peer: cbuf.at[pl.ds(peer * nb, nb)], lambda k: crec.at[k])
+                   lambda peer: cbuf.at[pl.ds(peer * nb, nb)], lambda k: crec.at[k], start=False)
+    for k in list(range(1, n_kv)) + [0]:
+        for i in range(nb):
+            attend(lax.rem(mk + k, n_kv) * nb + i)
+        if k > 0:
+            c_c[k - 1].start()
     pending += c_c
     for c in c_c:
         c.wait_recv()
@@ -223,32 +226,64 @@
         mine[t] = after[:, t * lanes:(t + 1) * lanes]
     mid = (after * mg_ref[...]).astype(BF16)
     mid_square = jnp.sum(after * after, axis=1, keepdims=True)
+    eye = lax.broadcasted_iota(jnp.int32, (batch, 128), 0) == lax.broadcasted_iota(jnp.int32, (batch, 128), 1)
+    sq_own[...] = jnp.sum(jnp.where(eye, mid_square, 0.0), axis=0, keepdims=True)
+    c_s = exchange("kv", n_kv, mk, kv_send.at[6], kv_recv.at[6], lambda peer: sq_own, lambda k: srec.at[k])
+    pending += c_s
     ld_g.wait()
-    gbuf[:, :, 0:ff] = jnp.dot(mid, wg[...], preferred_element_type=F32).reshape(batch, 1, ff)
     ld_u.wait()
-    gbuf[:, :, ff:2 * ff] = jnp.dot(mid, wu[...], preferred_element_type=F32).reshape(batch, 1, ff)
-    gbuf[:, :, 2 * ff:] = jnp.broadcast_to(mid_square, (batch, 128)).reshape(batch, 1, 128)
+    chunk = ubuf.shape[2]
     c_g = exchange("kv", n_kv, mk, kv_send.at[4], kv_recv.at[4],
-                   lambda peer: gbuf.at[pl.ds(peer * nb, nb)], lambda k: grec.at[k])
+                   lambda peer: gbuf.at[peer], lambda k: grec.at[k], start=False)
     pending += c_g
-    for c in c_g:
-        c.wait_recv()
-    for i in range(nb):
-        total = gbuf[mk * nb + i]
-        for k in range(1, n_kv):
-            total = total + grec[k, i]
-        inv = lax.rsqrt(total[:, 2 * ff:2 * ff + 1] / d_model + norm_eps)
-        gate = total[:, 0:ff] * inv
-        up = total[:, ff:2 * ff] * inv
-        ubuf[mk * nb + i] = gate / (1.0 + jnp.exp(-gate)) * up
+    for s in range(n_kv):
+        low = s * chunk
+        size = max(0, min(ff - low, chunk))
+        for at, weight in ((0, wg), (chunk, wu)):
+            if size > 0:
+                gbuf[s, :, at:at + size] = jnp.dot(
+                    mid, weight[:, low:low + size], preferred_element_type=F32).astype(BF16)
+            if size < chunk:
+                gbuf[s, :, at + size:at + chunk] = jnp.zeros((batch, chunk - size), BF16)
+
+        @pl.when(mk != s)
+        def _():
+            k = lax.rem(s - mk + n_kv, n_kv)
+            pltpu.make_async_remote_copy(
+                src_ref=gbuf.at[s],
+                dst_ref=grec.at[k],
+                send_sem=kv_send.at[4, k],
+                recv_sem=kv_recv.at[4, k],
+                device_id={"kv": jnp.int32(s)},
+                device_id_type=MESH,
+            ).start()
+
+    squares = sq_own[...]
+    for k in range(1, n_kv):
+        c_s[k - 1].wait_recv()
+        squares = squares + srec[k]
+    squares = jnp.sum(jnp.where(eye, jnp.broadcast_to(squares, eye.shape), 0.0), axis=1, keepdims=True)
+    mid_inv = lax.rsqrt(squares / d_model + norm_eps)
+    total = gbuf[mk].astype(F32)
+    for k in range(1, n_kv):
+        c_g[k - 1].wait_recv()
+        total = total + grec[k].astype(F32)
+    gate = total[:, 0:chunk] * mid_inv
+    up = total[:, chunk:] * mid_inv
+    ubuf[mk] = (gate / (1.0 + jnp.exp(-gate)) * up).astype(BF16)
     c_u = exchange("kv", n_kv, mk, kv_send.at[5], kv_recv.at[5],
-                   lambda peer: ubuf.at[own_rows], lambda k: ubuf.at[own_rows])
+                   lambda peer: ubuf.at[mk], lambda k: ubuf.at[mk])
     pending += c_u
     ld_d.wait()
     for c in c_u:
         c.wait_recv()
-    units = ubuf[:, 0, :].astype(BF16)
-    down = jnp.dot(units, wd[...], preferred_element_type=F32).astype(BF16)
+    down = jnp.zeros((batch, wd.shape[1]), F32)
+    for s in range(n_kv):
+        low = s * chunk
+        size = max(0, min(ff - low, chunk))
+        if size > 0:
+            down = down + jnp.dot(ubuf[s][:, 0:size], wd[low:low + size, :], preferred_element_type=F32)
+    down = down.astype(BF16)
     for t in range(n_tp):
         dbuf[t] = down[:, t * lanes:(t + 1) * lanes]
     c_d = exchange("tp", n_tp, mt, tp_send.at[2], tp_recv.at[2], lambda peer: dbuf.at[peer], lambda k: drec.at[k])
@@ -279,7 +314,7 @@
     rows = max(16, -(-kvh * span // 16) * 16)
     nb = batch // n_kv
     width = nq + 2 * nk + 128
-    wide = 2 * ff + 128
+    chunk = -(-ff // (128 * n_kv)) * 128
     vmem = pl.BlockSpec(memory_space=pltpu.VMEM)
     anywhere = pl.BlockSpec(memory_space=pl.ANY)
     big = (w_query, w_key, w_value, key_cache, value_cache, decay_to_end, w_output, w_gate, w_up, w_down)
@@ -295,16 +330,18 @@
         pltpu.VMEM((n_kv, nb, span, nk), F32),
         pltpu.VMEM((batch, span, nk), F32),
         pltpu.VMEM((n_tp, batch, w_output.shape[1]), BF16),
-        pltpu.VMEM((batch, 1, wide), F32),
-        pltpu.VMEM((n_kv, nb, 1, wide), F32),
-        pltpu.VMEM((batch, 1, ff), F32),
+        pltpu.VMEM((n_kv, batch, 2 * chunk), BF16),
+        pltpu.VMEM((n_kv, batch, 2 * chunk), BF16),
+        pltpu.VMEM((n_kv, batch, chunk), BF16),
+        pltpu.VMEM((1, 128), F32),
+        pltpu.VMEM((n_kv, 1, 128), F32),
         pltpu.VMEM((n_tp, batch, lanes), BF16),
         pltpu.VMEM((n_tp, batch, lanes), BF16),
         pltpu.VMEM((n_tp, batch, lanes), F32),
         pltpu.SemaphoreType.DMA((9,)),
         pltpu.SemaphoreType.DMA((kvh * group,)),
-        pltpu.SemaphoreType.DMA((6, n_kv)),
-        pltpu.SemaphoreType.DMA((6, n_kv)),
+        pltpu.SemaphoreType.DMA((7, n_kv)),
+        pltpu.SemaphoreType.DMA((7, n_kv)),
         pltpu.SemaphoreType.DMA((3, n_tp)),
         pltpu.SemaphoreType.DMA((3, n_tp)),
     ]
@@ -318,7 +355,7 @@
             collective_id=0, has_side_effects=True, vmem_limit_bytes=60 * 1024 * 1024
         ),
         name="decode_layer",
-    )(hidden_in, pre_gain.reshape(1, -1), w_forget, mid_gain.reshape(1, -1), forget_bias, *big)
+    )(hidden_in, pre_gain.reshape(1, -1), w_forget.T, mid_gain.reshape(1, -1), forget_bias, *big)
 
 
 def solution(mesh):

time: 63.2 us -> 58.3 us (0.922)
  Pallas kernels: 60.1 us -> 56.7 us
  local copies, waits for them, and re-layouts: 2.75 us -> 1.3 us
    pallas_call x1, Pallas kernels: 60.1 us -> 56.7 us  [on_device(): pl.pallas_call(functools.partial(layer_kernel, n_kv, n_tp, group, d_model...]
    unnamed x2 -> x1, local copies, waits for them, and re-layouts: 2.75 us -> 1.3 us
where the time goes in v2:
time: 58.3 us; the launch traced here: 58.1 us
  Pallas kernels  56.7 us (97%)
  local copies, waits for them, and re-layouts  1.3 us (2%)
    pallas_call x1, Pallas kernels, on_device(): pl.pallas_call(functools.partial(layer_kernel, n_kv, n_tp, group, d_model...  56.7 us
    unnamed x1, local copies, waits for them, and re-layouts  1.3 us

profile of v2, /device:TPU:0, one launch (start us, length us, event | category | flops | bytes accessed | tf_op | source)
XLA Modules:
  0.0 58.1 jit_solution(12845550358141128689)
XLA Ops:
  0.0 56.7 %decode_layer.1 = f32[16,128]{1,0:T(8,128)} custom-call(bf16[16,128]{1,0:T(8,128)(2,1)} %hid_ref.1, f32[1,512]{1,0:T(1,128)} %bitcast.4, bf16[16,512]{1,0:T(8,128)(2,1)} %bitcast.3, f32[1,512]{1,0:T(1,128)} %bitcast.5, f32[4]{0:T(128)} %bias_ref.1, bf16[512,768]{1,0:T(8,128)(2,1)} %wq_hbm.1, bf16[512,256]{1,0:T(8,128)(2,1)} %wk_hbm.1, ...), custom_call_target="tpu_custom_call" | custom-call | tf_op jit(solution)/shard_map/decode_layer/pallas_call | solution.py:348
  56.8 1.3 %copy.17 = f32[16,128]{1,0:T(8,128)} copy(f32[16,128]{1,0:T(8,128)} %decode_layer.1) | data formatting | bytes 16384
